TPU v7x, 32 devices: a whole 2x2x4 slice. The times are simulated.
32 devices in a mesh: ep: 8 (over z, x), tp: 4 (over y, core).
Axes of the slice: x: 2, y: 2, z: 4, core: 2. Of those that a mesh axis runs over, the one named last changes fastest.
Arguments:
- mix_in: bfloat16 [1024, 2048], P('ep'), may hold values from -6 to 6
- mix_gain: float32 [2048], replicated, may hold values from 0.1 to 1.9
- query_weight: bfloat16 [2048, 3072], P(None, 'tp'), may hold values from -0.125 to 0.125
- latent_weight: bfloat16 [2048, 512], replicated, may hold values from -0.125 to 0.125
- rotary_weight: bfloat16 [2048, 64], replicated, may hold values from -0.125 to 0.125
- latent_gain: float32 [512], replicated, may hold values from 0.1 to 1.9
- key_weight: bfloat16 [512, 2048], P(None, 'tp'), may hold values from -0.25 to 0.25
- value_weight: bfloat16 [512, 2048], P(None, 'tp'), may hold values from -0.25 to 0.25
- output_weight: bfloat16 [2048, 2048], P('tp'), may hold values from -0.125 to 0.125
- out_gain: float32 [2048], replicated, may hold values from 0.1 to 1.9
- ffn_in: bfloat16 [1024, 2048], P('ep'), may hold values from -6 to 6
- ffn_gain: float32 [2048], replicated, may hold values from 0.1 to 1.9
- gate_weight: bfloat16 [8, 2048, 1024], P('ep', None, 'tp'), may hold values from -0.375 to 0.375
- up_weight: bfloat16 [8, 2048, 1024], P('ep', None, 'tp'), may hold values from -0.375 to 0.375
- down_weight: bfloat16 [8, 1024, 2048], P('ep', 'tp'), may hold values from -0.046875 to 0.046875
- routes: int32 [1024, 4], P('ep'), may hold values from 0 to 7, all different within a row; in each aligned block of 32 rows (0 to 31, 32 to 63, ...) at most 32 rows name the same one
- route_scores: float32 [1024, 4], P('ep'), may hold values from -6 to 6
Outputs:
- mixed: bfloat16 [1024, 2048], P(('ep', 'tp'))
- moe_out: bfloat16 [1024, 2048], P(('ep', 'tp'))
Inputs may be any that keep to these rules, and one draw needn't show every extreme that they name: `routes`: each row names 4 different experts; in each aligned block of 32 rows no expert is named by more than 32 rows, a bound that some blocks reach.
All inputs are finite; a program needn't handle non-finite values.
Results may differ from a plain program's by a relative error of at most 0.014.
Values may be sent and summed in bfloat16 or wider, within the bound.
No kernel may reach another device: no remote copies, remote signals or barrier semaphores. Data moves between devices by JAX's collectives and lax.ppermute only.
A program may use at most 192 MiB of HBM per device.

v0:
```python
import jax
import jax.numpy as jnp
from jax import lax
from jax.sharding import PartitionSpec as P

NOPE = 128
ROPE = 64
VD = 128
norm_eps = 1e-06
clamp_limit = 7.0
gate_slope = 1.702
rope_base = 10000.0


def rms_rows(rows_in, scales):
    mean_square = jnp.mean(rows_in * rows_in, axis=-1, keepdims=True)
    return rows_in * lax.rsqrt(mean_square + norm_eps) * scales


def rms_columns(columns, scales):
    mean_square = jnp.mean(columns * columns, axis=0, keepdims=True)
    return columns * lax.rsqrt(mean_square + norm_eps) * scales[:, None]


def turn_table(positions):
    inverse = rope_base ** (-jnp.arange(0, ROPE, 2).astype(jnp.float32) / ROPE)
    angle_rows = inverse[:, None] * positions.astype(jnp.float32)[None, :]
    return (jnp.cos(angle_rows), jnp.sin(angle_rows))


def clamped_unit(gate_part, linear):
    gate_part = jnp.minimum(gate_part, clamp_limit)
    linear = jnp.clip(linear, -clamp_limit, clamp_limit)
    return gate_part * jax.nn.sigmoid(gate_slope * gate_part) * (linear + 1.0)


def keep_state(running):
    return running


def local(
    mix_in,
    mix_gain,
    query_weight,
    latent_weight,
    rotary_weight,
    latent_gain,
    key_weight,
    value_weight,
    output_weight,
    out_gain,
    ffn_in,
    ffn_gain,
    gate_weight,
    up_weight,
    down_weight,
    routes,
    route_scores,
):
    row_count = mix_in.shape[0]
    first_row = lax.axis_index("ep") * row_count
    last_row = first_row + row_count - 1
    positions = first_row + jnp.arange(row_count, dtype=jnp.int32)
    normed = rms_rows(mix_in.astype(jnp.float32), mix_gain).astype(jnp.bfloat16)
    head_count = query_weight.shape[1] // (NOPE + ROPE)
    half_rope = ROPE // 2
    cosine, sine_rows = turn_table(positions)
    queries = jnp.dot(normed, query_weight, preferred_element_type=jnp.float32).reshape(
        row_count, head_count, NOPE + ROPE
    )
    query_plain = queries[..., :NOPE].astype(jnp.bfloat16)
    query_cos = cosine.T[:, None, :]
    query_sin = sine_rows.T[:, None, :]
    query_upper = queries[..., NOPE : NOPE + half_rope]
    query_lower = queries[..., NOPE + half_rope :]
    query_turn = jnp.concatenate(
        [
            query_upper * query_cos - query_lower * query_sin,
            query_lower * query_cos + query_upper * query_sin,
        ],
        axis=-1,
    ).astype(jnp.bfloat16)
    across = (((0,), (1,)), ((), ()))
    latent = rms_columns(
        lax.dot_general(latent_weight, normed, across, preferred_element_type=jnp.float32),
        latent_gain,
    ).astype(jnp.bfloat16)
    rot_raw = lax.dot_general(rotary_weight, normed, across, preferred_element_type=jnp.float32)
    rotary_key = jnp.concatenate(
        [
            rot_raw[:half_rope] * cosine - rot_raw[half_rope:] * sine_rows,
            rot_raw[half_rope:] * cosine + rot_raw[:half_rope] * sine_rows,
        ],
        axis=0,
    ).astype(jnp.bfloat16)
    score_scale = (NOPE + ROPE) ** (-0.5)
    contract_first = (((0,), (0,)), ((), ()))

    def expand(latent_block):
        key_block = lax.dot_general(
            key_weight, latent_block, contract_first, preferred_element_type=jnp.float32
        ).astype(jnp.bfloat16)
        value_block = lax.dot_general(
            value_weight, latent_block, contract_first, preferred_element_type=jnp.float32
        ).astype(jnp.bfloat16)
        return (key_block, value_block)

    def attend(key_block, value_block, turn_block):
        key_count = key_block.shape[1]
        key_block = key_block.reshape(head_count, NOPE, key_count)
        value_block = value_block.reshape(head_count, VD, key_count)
        scores = jnp.einsum(
            "ihd,hdj->hij", query_plain, key_block, preferred_element_type=jnp.float32
        )
        scores = scores + jnp.einsum(
            "ihd,dj->hij", query_turn, turn_block, preferred_element_type=jnp.float32
        )
        key_places = jnp.arange(key_count, dtype=jnp.int32)
        allowed = key_places[None, :] <= positions[:, None]
        weights = jnp.where(allowed[None], jnp.exp(scores * score_scale), 0.0)
        weighted = jnp.einsum(
            "hij,hdj->hid",
            weights.astype(jnp.bfloat16),
            value_block,
            preferred_element_type=jnp.float32,
        )
        return (jnp.sum(weights, axis=-1), weighted)

    initial = (
        jnp.zeros((head_count, row_count), jnp.float32),
        jnp.zeros((head_count, row_count, VD), jnp.float32),
    )
    shard_piece = (
        lax.all_gather(latent, "ep", axis=1, tiled=True),
        lax.all_gather(rotary_key, "ep", axis=1, tiled=True),
    )

    def compute_piece(running):
        key_block, value_block = expand(shard_piece[0])
        return attend(key_block, value_block, shard_piece[1])

    totals, weighted = lax.cond(jnp.int32(0) > last_row, keep_state, compute_piece, initial)
    attended = (weighted / totals[..., None]).astype(jnp.bfloat16)
    mixing = output_weight.reshape(head_count, VD, output_weight.shape[1])
    partial_value = jnp.einsum("hid,hde->ie", attended, mixing, preferred_element_type=jnp.float32)
    projected = lax.psum_scatter(
        lax.optimization_barrier(partial_value.astype(jnp.bfloat16))
        .astype(jnp.float32)
        .astype(jnp.bfloat16),
        "tp",
        scatter_dimension=0,
        tiled=True,
    ).astype(jnp.float32)
    mixed = rms_rows(projected, out_gain).astype(jnp.bfloat16)
    tokens = ffn_in.shape[0]
    part_count = lax.axis_size("tp")
    quarter_rows = tokens // part_count
    experts = lax.axis_size("ep")
    choose = routes.shape[1]
    capacity = max(2, 2 * quarter_rows * choose // experts)
    slot_count = capacity * part_count
    tp_index = lax.axis_index("tp")
    normed_b = rms_rows(ffn_in.astype(jnp.float32), ffn_gain).astype(jnp.bfloat16)
    padded = jnp.concatenate([normed_b, jnp.zeros((1, normed_b.shape[1]), jnp.bfloat16)], axis=0)
    gate_share = jax.nn.softmax(route_scores, axis=-1)
    grouped = routes.reshape(part_count, quarter_rows * choose)
    onehot = (grouped[:, :, None] == jnp.arange(experts, dtype=jnp.int32)[None, None, :]).astype(
        jnp.int32
    )
    slot_rank = jnp.sum((jnp.cumsum(onehot, axis=1) - 1) * onehot, axis=2)
    slot_index = jnp.arange(part_count, dtype=jnp.int32)[:, None] * capacity + slot_rank
    place_index = (slot_index * experts + grouped).reshape(-1)
    owners = jnp.arange(tokens * choose, dtype=jnp.int32) // choose
    slot_token = jnp.full((slot_count * experts,), tokens, jnp.int32).at[place_index].set(owners)
    unit_count = gate_weight.shape[2]
    chosen = lax.dynamic_slice_in_dim(
        slot_token, tp_index * capacity * experts, capacity * experts, 0
    )
    outgoing = padded[chosen].reshape(capacity, experts, -1)
    arrived = lax.all_to_all(outgoing, "ep", split_axis=1, concat_axis=1, tiled=True)
    row_block = lax.all_gather(arrived, "tp", axis=0, tiled=True)
    block_slots = row_block.shape[0]
    flat_rows = row_block.reshape(-1, row_block.shape[2])
    gate_part = jnp.dot(flat_rows, gate_weight[0], preferred_element_type=jnp.float32)
    up_part = jnp.dot(flat_rows, up_weight[0], preferred_element_type=jnp.float32)
    hidden = (
        clamped_unit(gate_part, up_part).astype(jnp.bfloat16).reshape(block_slots, -1, unit_count)
    )
    sources = hidden.shape[1]
    hidden_flat = hidden.reshape(slot_count * sources, unit_count)
    partial_value = jnp.dot(hidden_flat, down_weight[0], preferred_element_type=jnp.float32)
    result = lax.psum_scatter(
        lax.optimization_barrier(partial_value.astype(jnp.bfloat16))
        .astype(jnp.float32)
        .astype(jnp.bfloat16),
        "tp",
        scatter_dimension=0,
        tiled=True,
    )
    result = result.reshape(capacity, sources, -1)
    returned = lax.all_to_all(result, "ep", split_axis=1, concat_axis=1, tiled=True)
    back_rows = returned.reshape(capacity * experts, -1)
    own_rank = lax.dynamic_index_in_dim(slot_rank, tp_index, 0, keepdims=False)
    own_expert = lax.dynamic_index_in_dim(grouped, tp_index, 0, keepdims=False)
    picked = (
        back_rows[own_rank * experts + own_expert]
        .astype(jnp.float32)
        .reshape(quarter_rows, choose, -1)
    )
    own_gates = lax.dynamic_slice_in_dim(gate_share, tp_index * quarter_rows, quarter_rows, 0)
    moe_out = jnp.sum(picked * own_gates[:, :, None], axis=1).astype(jnp.bfloat16)
    return (mixed, moe_out)


def solution(mesh):
    placed = (
        P("ep", None),
        P(),
        P(None, "tp"),
        P(),
        P(),
        P(),
        P(None, "tp"),
        P(None, "tp"),
        P("tp", None),
        P(),
        P("ep", None),
        P(),
        P("ep", None, "tp"),
        P("ep", None, "tp"),
        P("ep", "tp", None),
        P("ep", None),
        P("ep", None),
    )
    return jax.shard_map(
        local,
        mesh=mesh,
        in_specs=placed,
        out_specs=(P(("ep", "tp"), None), P(("ep", "tp"), None)),
        check_vma=False,
    )
```

profile of v0, /device:TPU:0, one launch (start us, length us, event | category | flops | bytes accessed | tf_op | source)
XLA Modules:
  0.0 232.8 jit_solution(3613812320336969351)
XLA Ops:
  10.8 2.5 %scatter_custom_fusion = s32[1024]{0:T(1024)S(1)} fusion(s32[512]{0:T(512)S(1)} %bitcast.86, s32[512]{0:T(512)S(1)} %add_select_fusion, s32[]{:T(128)} %constant.36.clone.1), kind=kCustom, calls=%fused_computation.95 | custom fusion | bytes 4100 | tf_op jit(solution)/shard_map/scatter | solution.py:174
  16.7 4.5 %gather_fusion = bf16[256,2048]{1,0:T(8,128)(2,1)} fusion(bf16[129,2048]{1,0:T(8,128)(2,1)} %concatenate.13, s32[1024]{0:T(1024)S(1)} %pad_clamp_fusion.1), kind=kCustom, calls=%fused_computation | custom fusion | bytes 2098176 | tf_op jit(solution)/shard_map/gather | solution.py:179
  21.2 1.8 copy.43
  23.0 32.8 %all_to_all.10 = bf16[32,8,2048]{2,0,1:T(8,128)(2,1)S(1)} all-to-all(bf16[32,8,2048]{2,0,1:T(8,128)(2,1)S(1)} %copy.43), channel_id=1, replica_groups=mesh['ep'=8,'tp'=4] {'ep'}, dimensions={1} | all-to-all | bytes 2097152 | tf_op jit(solution)/shard_map/all_to_all | solution.py:180
  58.7 2.3 %multiply_reduce_fusion.1 = (f32[128]{0:T(128)S(1)}, f32[128,512]{1,0:T(8,128)S(1)}) fusion(bf16[2048,512]{1,0:T(8,128)(2,1)} %param.22, bf16[128,2048]{1,0:T(8,128)(2,1)} %param.19, f32[2048]{0:T(1024)S(1)} %copy-done.4, f32[128]{0:T(128)S(1)} %add_rsqrt_fusion.3), kind=kOutput, calls=%fused_computation.63 | convolution fusion | flops 269614976 | bytes 2892800 | tf_op jit(solution)/shard_map/dot_general | solution.py:85
  61.9 29.2 %all-gather.5.cloned.1.call-done = bf16[128,8,2048]{2,1,0:T(8,128)(2,1)} async-done(((bf16[32,8,2048]{2,1,0:T(8,128)(2,1)}), bf16[128,8,2048]{2,1,0:T(8,128)(2,1)}) %all-gather.5.cloned.1.call-update) | async-done | bytes 4194320 | tf_op jit(solution)/shard_map/all_gather | solution.py:181
  91.1 4.7 %fusion.12 = f32[1024,256]{1,0:T(8,128)} fusion(bf16[128,8,2048]{2,1,0:T(8,128)(2,1)} %all-gather.5.cloned.1.call-done, bf16[1,2048,256]{2,1,0:T(8,128)(2,1)} %param.31), kind=kOutput, calls=%fused_computation.22 | convolution fusion | flops 1074003968 | bytes 6291456 | tf_op jit(solution)/shard_map/dot_general | solution.py:184
  95.8 9.4 %convolution_convert_fusion.2 = bf16[1024,2048]{1,0:T(8,128)(2,1)} fusion(bf16[128,8,2048]{2,1,0:T(8,128)(2,1)} %all-gather.5.cloned.1.call-done, bf16[1,256,2048]{2,1,0:T(8,128)(2,1)} %param.33, bf16[1,2048,256]{2,1,0:T(8,128)(2,1)} %param.32, f32[1024,256]{1,0:T(8,128)} %fusion.12), kind=kOutput, calls=%fused_computation.19 | convolution fusion | flops 2151940096 | bytes 11534336 | tf_op jit(solution)/shard_map/dot_general | solution.py:191
  107.7 27.7 %all_gather.10 = bf16[64,1024]{1,0:T(8,128)(2,1)} all-gather(bf16[64,128]{1,0:T(8,128)(2,1)S(1)} %pad_maximum_fusion.1), channel_id=1, replica_groups=mesh['ep'=8,'tp'=4] {'ep'}, dimensions={1}, use_global_device_ids=true | all-gather | bytes 147456 | tf_op jit(solution)/shard_map/all_gather | solution.py:135
  136.1 2.4 %fusion.79 = f32[128,768]{0,1:T(8,128)S(1)} fusion(bf16[2048,768]{1,0:T(8,128)(2,1)S(1)} %copy-done, bf16[128,2048]{1,0:T(8,128)(2,1)} %param.19, f32[2048]{0:T(1024)S(1)} %copy-done.4, f32[128]{0:T(128)} %copy-done.7), kind=kOutput, calls=%fused_computation.118 | convolution fusion | flops 403701760 | bytes 4071936 | tf_op jit(solution)/shard_map/dot_general | solution.py:68
  139.2 8.9 %conditional.1 = (f32[4,128]{1,0:T(4,128)S(1)}, f32[4,128,128]{2,1,0:T(8,128)S(1)}) conditional(s32[]{:T(128)} %convert_element_type.84, (s32[128]{0:T(128)}, bf16[512,512]{1,0:T(8,128)(2,1)}, bf16[512,1024]{0,1:T(8,128)(2,1)}, f32[128,4,192]{0,2,1:T(8,128)S(1)}, bf16[64,1024]{1,0:T(8,128)(2,1)}, /*index=5*/bf16[128,4,64]{0,2,1:T(8,128)(2,1)}, ...), branch_computations={%region_2.4_spmd, %region_4.5_spmd} | conditional | flops 1413086720 | bytes 22155932 | solution.py:142
  139.2 3.2 %convolution_convert_fusion.1 = bf16[512,1024]{1,0:T(8,128)(2,1)} fusion(bf16[512,512]{1,0:T(8,128)(2,1)} %get-tuple-element.30, bf16[512,1024]{0,1:T(8,128)(2,1)} %get-tuple-element.49), kind=kOutput, calls=%fused_computation.8 | convolution fusion | flops 537395200 | bytes 2621440 | tf_op jit(solution)/shard_map/cond/branch_0_fun/dot_general | solution.py:100
  143.2 2.1 fusion.5
  148.1 2.9 %fusion.11 = bf16[128,2048]{1,0:T(8,128)(2,1)} fusion(bf16[4,128,2048]{2,1,0:T(8,128)(2,1)} %bitcast.81, f32[4,128,128]{2,1,0:T(8,128)S(1)} %get-tuple-element.25, f32[4,128]{1,0:T(4,128)S(1)} %get-tuple-element.26), kind=kOutput, calls=%fused_computation.21 | convolution fusion | flops 268828672 | bytes 2885632 | tf_op jit(solution)/shard_map/hid,hde->ie/dot_general | solution.py:145
  151.0 29.7 %reduce-scatter.5.cloned.1.call-done = bf16[256,2048]{1,0:T(8,128)(2,1)} async-done(((bf16[1024,2048]{1,0:T(8,128)(2,1)}), bf16[256,2048]{1,0:T(8,128)(2,1)}) %reduce-scatter.5.cloned.1.call-update) | async-done | bytes 1048592 | tf_op jit(solution)/shard_map/reduce_scatter | solution.py:192
  180.7 2.9 %copy.45 = bf16[32,8,2048]{2,0,1:T(8,128)(2,1)} copy(bf16[32,8,2048]{2,1,0:T(8,128)(2,1)} %bitcast.83) | data formatting | bytes 2097152 | tf_op jit(solution)/shard_map/reshape | solution.py:200
  183.6 5.5 %all-to-all-start.1 = ((bf16[32,8,2048]{2,0,1:T(8,128)(2,1)}), bf16[32,8,2048]{2,0,1:T(8,128)(2,1)}, u32[]{:S(2)}, u32[]{:S(2)}) async-start(bf16[32,8,2048]{2,0,1:T(8,128)(2,1)} %copy.45), calls=%async_computation.3 | async-start | bytes 2097152 | tf_op jit(solution)/shard_map/all_to_all | solution.py:201
  189.4 15.4 %reduce-scatter.3.cloned.1.call-done = bf16[32,2048]{1,0:T(8,128)(2,1)} async-done(((bf16[128,2048]{1,0:T(8,128)(2,1)}), bf16[32,2048]{1,0:T(8,128)(2,1)}) %reduce-scatter.3.cloned.1.call-update) | async-done | bytes 131088 | tf_op jit(solution)/shard_map/reduce_scatter | solution.py:146
  205.8 1.7 fusion.51
  207.5 7.4 %all-to-all-done.1 = bf16[32,8,2048]{2,0,1:T(8,128)(2,1)} async-done(((bf16[32,8,2048]{2,0,1:T(8,128)(2,1)}), bf16[32,8,2048]{2,0,1:T(8,128)(2,1)}, u32[]{:S(2)}, u32[]{:S(2)}) %all-to-all-start.1) | async-done | bytes 1048608 | tf_op jit(solution)/shard_map/all_to_all | solution.py:201
  214.9 2.8 %copy.53 = bf16[32,8,2048]{2,1,0:T(8,128)(2,1)} copy(bf16[32,8,2048]{2,0,1:T(8,128)(2,1)} %all-to-all-done.1) | data formatting | bytes 2097152 | tf_op jit(solution)/shard_map/all_to_all | solution.py:201
  217.7 3.6 %gather_fusion.1 = bf16[128,2048]{1,0:T(8,128)(2,1)} fusion(bf16[256,2048]{1,0:T(8,128)(2,1)} %bitcast.77, s32[1024]{0:T(1024)S(1)} %pad_clamp_fusion), kind=kCustom, calls=%fused_computation.1 | custom fusion | bytes 1049088 | tf_op jit(solution)/shard_map/gather | solution.py:206
  221.3 2.4 %reshape.248 = f32[32,4,2048]{2,1,0:T(4,128)} reshape(bf16[128,2048]{1,0:T(8,128)(2,1)} %gather_fusion.1) | data formatting | bytes 1572864 | tf_op jit(solution)/shard_map/convert_element_type | solution.py:207
  223.7 2.6 %multiply_reduce_fusion = bf16[32,2048]{1,0:T(8,128)(2,1)} fusion(f32[32,4,2048]{2,1,0:T(4,128)} %reshape.248, f32[32,4]{1,0:T(8,128)S(1)} %copy.47), kind=kLoop, calls=%fused_computation.42 | loop fusion | flops 458752 | bytes 1180160 | tf_op jit(solution)/shard_map/reduce_sum | solution.py:211
  (77 shorter events, 19.4 us)
Async XLA Ops:
  7.2 128.9 %copy-start = (bf16[2048,768]{1,0:T(8,128)(2,1)S(1)}, bf16[2048,768]{1,0:T(8,128)(2,1)}, u32[]{:S(2)}) copy-start(bf16[2048,768]{1,0:T(8,128)(2,1)} %param.21) | copy-start | bytes 9437188
  7.2 83.9 %all-gather.5.cloned.1.call-start = ((), (), s32[]{:S(2)}) async-start(), calls=%async_computation.6 | async-start | bytes 5242880 | tf_op jit(solution)/shard_map/all_gather | solution.py:181
  55.8 2.9 %copy-start.4 = (f32[2048]{0:T(1024)S(1)}, f32[2048]{0:T(1024)}, u32[]{:S(2)}) copy-start(f32[2048]{0:T(1024)} %param.20) | copy-start | bytes 24580
  57.4 3.7 %copy-start.6 = (f32[512]{0:T(512)S(1)}, f32[512]{0:T(512)}, u32[]{:S(2)}) copy-start(f32[512]{0:T(512)} %param.24) | copy-start | bytes 6148
  57.4 81.8 %all-gather.3.cloned.1.call-start = ((), (), s32[]{:S(2)}) async-start(), calls=%async_computation.4 | async-start | bytes 1179648 | tf_op jit(solution)/shard_map/all_gather | solution.py:134
  58.7 46.6 %copy-start.7 = (f32[128]{0:T(128)}, f32[128]{0:T(128)S(1)}, u32[]{:S(2)}) copy-start(f32[128]{0:T(128)S(1)} %add_rsqrt_fusion.3) | copy-start | bytes 1540
  61.8 118.9 %reduce-scatter.5.cloned.1.call-start = ((), (), s32[]{:S(2)}) async-start(), calls=%async_computation.7 | async-start | bytes 5242880 | tf_op jit(solution)/shard_map/reduce_scatter | solution.py:192
  105.2 0.9 copy-start.11
  105.2 99.6 %reduce-scatter.3.cloned.1.call-start = ((), (), s32[]{:S(2)}) async-start(), calls=%async_computation.5 | async-start | bytes 655360 | tf_op jit(solution)/shard_map/reduce_scatter | solution.py:146
  142.4 3.0 %copy-start.8 = (s32[128]{0:T(128)S(1)}, s32[128]{0:T(128)}, u32[]{:S(2)}) copy-start(s32[128]{0:T(128)} %get-tuple-element.14) | copy-start | bytes 1540 | tf_op jit(solution)/shard_map/cond
  143.2 2.3 copy-start.1
  143.2 2.3 copy-start.2
  145.3 1.3 copy-start.9
  145.4 1.5 copy-start.10
  180.7 8.4 %copy-start.3 = (f32[128,4]{0,1:T(4,128)S(1)}, f32[128,4]{0,1:T(4,128)}, u32[]{:S(2)}) copy-start(f32[128,4]{0,1:T(4,128)} %param.35) | copy-start | bytes 6148
  180.7 25.1 %copy-start.5 = (f32[2048]{0:T(1024)S(1)}, f32[2048]{0:T(1024)}, u32[]{:S(2)}) copy-start(f32[2048]{0:T(1024)} %param.28) | copy-start | bytes 24580
  183.6 31.3 %all-to-all-start.1 = ((bf16[32,8,2048]{2,0,1:T(8,128)(2,1)}), bf16[32,8,2048]{2,0,1:T(8,128)(2,1)}, u32[]{:S(2)}, u32[]{:S(2)}) async-start(bf16[32,8,2048]{2,0,1:T(8,128)(2,1)} %copy.45), calls=%async_computation.3 | async-start | bytes 2097152 | tf_op jit(solution)/shard_map/all_to_all | solution.py:201
Sparse Core Ops, SparseCore 0:
  57.5 33.4 all-gather.4
  93.8 40.4 all-gather.2
  136.8 43.9 reduce-scatter.4
  183.1 21.6 reduce-scatter.2
where the time goes:
time: 234 us; the launch traced here: 233 us
  waiting for transfers between devices  81.7 us (35%)
  blocking collectives  60.5 us (26%)
  matrix products  30.5 us (13%)
  local copies, waits for them, and re-layouts  26.4 us (11%)
  between operations  14 us (6%)
  other arithmetic  13.9 us (6%)
  starting transfers between devices  5.68 us (2%)
    reduce_scatter x2, waiting for transfers between devices, local(): lax.psum_scatter(lax.optimization_barrier(partial_value.astype(jnp.bfloat...  45.1 us
    all_to_all x1, blocking collectives, local(): lax.all_to_all(outgoing, 'ep', split_axis=1, concat_axis=1, tiled=True)  32.8 us
    all_gather x1, waiting for transfers between devices, local(): row_block = lax.all_gather(arrived, 'tp', axis=0, tiled=True)  29.2 us
    all_gather x1, blocking collectives, local(): lax.all_gather(rotary_key, 'ep', axis=1, tiled=True)  27.7 us
    dot_general x1, matrix products, local(): jnp.dot(hidden_flat, down_weight[0], preferred_element_type=jnp.float32)  9.41 us
    all_to_all x1, waiting for transfers between devices, local(): lax.all_to_all(result, 'ep', split_axis=1, concat_axis=1, tiled=True)  7.37 us
    all_to_all x1, starting transfers between devices, local(): lax.all_to_all(result, 'ep', split_axis=1, concat_axis=1, tiled=True)  5.52 us
    dot_general x1, matrix products, local(): jnp.dot(flat_rows, gate_weight[0], preferred_element_type=jnp.float32)  4.72 us
  transfers between devices with their start and end apart: 5, of which 4 were waited for; matrix products, arithmetic and copies ran while one was open for 18% of the time, Pallas kernels for 0%

commit v1 on v0

--- a/solution.py
+++ b/solution.py
@@ -178,7 +178,12 @@
     )
     outgoing = padded[chosen].reshape(capacity, experts, -1)
     arrived = lax.all_to_all(outgoing, "ep", split_axis=1, concat_axis=1, tiled=True)
-    row_block = lax.all_gather(arrived, "tp", axis=0, tiled=True)
+    ring = [arrived]
+    for hop in range(3):
+        ring.append(lax.ppermute(ring[-1], "tp", [(dev, (dev + 1) % 4) for dev in range(4)]))
+    row_block = jnp.roll(
+        jnp.concatenate(ring[::-1], axis=0), (lax.axis_index("tp") + 1) * ring[0].shape[0], axis=0
+    )
     block_slots = row_block.shape[0]
     flat_rows = row_block.reshape(-1, row_block.shape[2])
     gate_part = jnp.dot(flat_rows, gate_weight[0], preferred_element_type=jnp.float32)

time: 234 us -> 224 us (0.957)
  waiting for transfers between devices: 81.7 us -> 59.5 us
  local copies, waits for them, and re-layouts: 26.4 us -> 38.2 us
    ppermute x0 -> x3, waiting for transfers between devices: none -> 38.4 us  [local(): lax.ppermute(ring[-1], 'tp', [(dev, (dev + 1) % 4) for dev in range(4)])]
    reduce_scatter x2, waiting for transfers between devices: 45.1 us -> 13.6 us  [local(): lax.psum_scatter(lax.optimization_barrier(partial_value.astype(jnp.bfloat...]
    all_gather x1 -> x0, waiting for transfers between devices: 29.2 us -> none  [local(): row_block = lax.all_gather(arrived, 'tp', axis=0, tiled=True)]
    unnamed x15 -> x30, local copies, waits for them, and re-layouts: 1.81 us -> 14.6 us
    dot_general x1, matrix products: 4.72 us -> 2.22 us  [local(): jnp.dot(flat_rows, gate_weight[0], preferred_element_type=jnp.float32)]
  transfers between devices with their start and end apart: 5 -> 7, of which waited for: 4 -> 5; matrix products, arithmetic and copies ran while one was open for 18% -> 22% of each run, Pallas kernels for 0% -> 0%
where the time goes in v1:
time: 224 us; the launch traced here: 223 us
  blocking collectives  60.2 us (27%)
  waiting for transfers between devices  59.5 us (27%)
  local copies, waits for them, and re-layouts  38.2 us (17%)
  matrix products  30.1 us (13%)
  between operations  15.8 us (7%)
  other arithmetic  14.7 us (7%)
  starting transfers between devices  4.6 us (2%)
    ppermute x3, waiting for transfers between devices, local(): lax.ppermute(ring[-1], 'tp', [(dev, (dev + 1) % 4) for dev in range(4)])  38.4 us
    all_to_all x1, blocking collectives, local(): lax.all_to_all(outgoing, 'ep', split_axis=1, concat_axis=1, tiled=True)  32.8 us
    all_gather x1, blocking collectives, local(): lax.all_gather(rotary_key, 'ep', axis=1, tiled=True)  27.4 us
    unnamed x30, local copies, waits for them, and re-layouts  14.6 us
    reduce_scatter x2, waiting for transfers between devices, local(): lax.psum_scatter(lax.optimization_barrier(partial_value.astype(jnp.bfloat...  13.6 us
    dot_general x1, matrix products, local(): jnp.dot(hidden_flat, down_weight[0], preferred_element_type=jnp.float32)  9.5 us
    all_to_all x1, waiting for transfers between devices, local(): lax.all_to_all(result, 'ep', split_axis=1, concat_axis=1, tiled=True)  7.51 us
    gather x1, local copies, waits for them, and re-layouts, local(): outgoing = padded[chosen].reshape(capacity, experts, -1)  4.5 us
  transfers between devices with their start and end apart: 7, of which 5 were waited for; matrix products, arithmetic and copies ran while one was open for 22% of the time, Pallas kernels for 0%

profile of v1, /device:TPU:0, one launch (start us, length us, event | category | flops | bytes accessed | tf_op | source)
XLA Modules:
  0.0 223.2 jit_solution(16077550728732987062)
XLA Ops:
  11.6 2.5 %scatter_custom_fusion = s32[1024]{0:T(1024)S(1)} fusion(s32[512]{0:T(512)S(1)} %bitcast.87, s32[512]{0:T(512)S(1)} %add_select_fusion, s32[]{:T(128)} %constant.54.clone.1), kind=kCustom, calls=%fused_computation.98 | custom fusion | bytes 4100 | tf_op jit(solution)/shard_map/scatter | solution.py:174
  17.5 4.5 %gather_fusion = bf16[256,2048]{1,0:T(8,128)(2,1)} fusion(bf16[129,2048]{1,0:T(8,128)(2,1)} %concatenate.19, s32[1024]{0:T(1024)S(1)} %pad_clamp_fusion.1), kind=kCustom, calls=%fused_computation | custom fusion | bytes 2098176 | tf_op jit(solution)/shard_map/gather | solution.py:179
  23.8 32.8 %all_to_all.10 = bf16[32,8,2048]{2,0,1:T(8,128)(2,1)S(1)} all-to-all(bf16[32,8,2048]{2,0,1:T(8,128)(2,1)S(1)} %copy.54), channel_id=1, replica_groups=mesh['ep'=8,'tp'=4] {'ep'}, dimensions={1} | all-to-all | bytes 2097152 | tf_op jit(solution)/shard_map/all_to_all | solution.py:180
  58.3 14.2 %collective-permute-done = bf16[32,8,2048]{2,1,0:T(8,128)(2,1)S(1)} collective-permute-done((bf16[32,8,2048]{2,1,0:T(8,128)(2,1)S(1)}, bf16[32,8,2048]{2,1,0:T(8,128)(2,1)S(1)}, u32[]{:S(2)}, u32[]{:S(2)}) %collective-permute-start) | collective-permute-done | bytes 1048608 | tf_op jit(solution)/shard_map/ppermute | solution.py:183
  73.6 14.3 %collective-permute-done.1 = bf16[32,8,2048]{2,1,0:T(8,128)(2,1)} collective-permute-done((bf16[32,8,2048]{2,1,0:T(8,128)(2,1)S(1)}, bf16[32,8,2048]{2,1,0:T(8,128)(2,1)}, u32[]{:S(2)}, u32[]{:S(2)}) %collective-permute-start.1) | collective-permute-done | bytes 1048608 | tf_op jit(solution)/shard_map/ppermute | solution.py:183
  89.1 2.3 %multiply_reduce_fusion.1 = (f32[128]{0:T(128)S(1)}, f32[128,512]{1,0:T(8,128)S(1)}) fusion(bf16[2048,512]{1,0:T(8,128)(2,1)} %param.22, bf16[128,2048]{1,0:T(8,128)(2,1)} %param.19, f32[2048]{0:T(1024)S(1)} %copy-done.7, f32[128]{0:T(128)S(1)} %add_rsqrt_fusion.3), kind=kOutput, calls=%fused_computation.58 | convolution fusion | flops 269614976 | bytes 2892800 | tf_op jit(solution)/shard_map/dot_general | solution.py:85
  92.6 9.9 %collective-permute-done.2 = bf16[32,8,2048]{2,1,0:T(8,128)(2,1)} collective-permute-done((bf16[32,8,2048]{2,1,0:T(8,128)(2,1)}, bf16[32,8,2048]{2,1,0:T(8,128)(2,1)}, u32[]{:S(2)}, u32[]{:S(2)}) %collective-permute-start.2) | collective-permute-done | bytes 1048608 | tf_op jit(solution)/shard_map/ppermute | solution.py:183
  111.4 3.2 %copy-done.5 = bf16[256,8,2048]{2,1,0:T(8,128)(2,1)} copy-done((bf16[256,8,2048]{2,1,0:T(8,128)(2,1)}, bf16[256,8,2048]{2,1,0:T(8,128)(2,1)S(1)}, u32[]{:S(2)}) %copy-start.5) | copy-done | bytes 8388632
  114.6 2.2 fusion.14
  116.9 9.5 %convolution_convert_fusion.2 = bf16[1024,2048]{1,0:T(8,128)(2,1)} fusion(bf16[1,256,2048]{2,1,0:T(8,128)(2,1)} %param.33, f32[1024,256]{1,0:T(8,128)} %fusion.14, bf16[256,8,2048]{2,1,0:T(8,128)(2,1)} %copy-done.5, s32[]{:T(128)S(6)} %select_n.61, bf16[1,2048,256]{2,1,0:T(8,128)(2,1)} %param.32), kind=kOutput, calls=%fused_computation.19 | convolution fusion | flops 2151940096 | bytes 11534340 | tf_op jit(solution)/shard_map/dot_general | solution.py:196
  128.1 27.4 %all_gather.7 = bf16[64,1024]{1,0:T(8,128)(2,1)} all-gather(bf16[64,128]{1,0:T(8,128)(2,1)S(1)} %pad_maximum_fusion.1), channel_id=1, replica_groups=mesh['ep'=8,'tp'=4] {'ep'}, dimensions={1}, use_global_device_ids=true | all-gather | bytes 147456 | tf_op jit(solution)/shard_map/all_gather | solution.py:135
  156.2 2.4 %fusion.77 = f32[128,768]{0,1:T(8,128)S(1)} fusion(bf16[2048,768]{1,0:T(8,128)(2,1)S(1)} %copy-done, bf16[128,2048]{1,0:T(8,128)(2,1)} %param.19, f32[2048]{0:T(1024)} %param.20, f32[128]{0:T(128)S(1)} %add_rsqrt_fusion.3), kind=kOutput, calls=%fused_computation.123 | convolution fusion | flops 403701760 | bytes 4071936 | tf_op jit(solution)/shard_map/dot_general | solution.py:68
  159.3 11.0 %conditional.1 = (f32[4,128]{1,0:T(4,128)S(1)}, f32[4,128,128]{2,1,0:T(8,128)S(1)}) conditional(s32[]{:T(128)} %convert_element_type.84, (s32[128]{0:T(128)}, bf16[512,512]{1,0:T(8,128)(2,1)}, bf16[512,1024]{0,1:T(8,128)(2,1)}, f32[128,4,192]{0,2,1:T(8,128)S(1)}, bf16[64,1024]{1,0:T(8,128)(2,1)}, /*index=5*/bf16[128,4,64]{0,2,1:T(8,128)(2,1)}, ...), branch_computations={%region_2.4_spmd, %region_4.5_spmd} | conditional | flops 1413086720 | bytes 15075856 | solution.py:142
  159.3 3.2 %convolution_convert_fusion.1 = bf16[512,1024]{1,0:T(8,128)(2,1)} fusion(bf16[512,512]{1,0:T(8,128)(2,1)} %get-tuple-element.30, bf16[512,1024]{0,1:T(8,128)(2,1)} %get-tuple-element.56), kind=kOutput, calls=%fused_computation.8 | convolution fusion | flops 537395200 | bytes 2621440 | tf_op jit(solution)/shard_map/cond/branch_0_fun/dot_general | solution.py:100
  167.6 2.2 convolution_convert_fusion
  170.3 2.9 %fusion.13 = bf16[128,2048]{1,0:T(8,128)(2,1)} fusion(bf16[4,128,2048]{2,1,0:T(8,128)(2,1)} %bitcast.82, f32[4,128,128]{2,1,0:T(8,128)S(1)} %get-tuple-element.25, f32[4,128]{1,0:T(4,128)S(1)} %get-tuple-element.26), kind=kOutput, calls=%fused_computation.23 | convolution fusion | flops 268828672 | bytes 2885632 | tf_op jit(solution)/shard_map/hid,hde->ie/dot_general | solution.py:145
  173.2 2.8 %copy.58 = bf16[32,8,2048]{2,0,1:T(8,128)(2,1)} copy(bf16[32,8,2048]{2,1,0:T(8,128)(2,1)} %bitcast.84) | data formatting | bytes 2097152 | tf_op jit(solution)/shard_map/reshape | solution.py:205
  176.1 4.2 %all-to-all-start.1 = ((bf16[32,8,2048]{2,0,1:T(8,128)(2,1)}), bf16[32,8,2048]{2,0,1:T(8,128)(2,1)}, u32[]{:S(2)}, u32[]{:S(2)}) async-start(bf16[32,8,2048]{2,0,1:T(8,128)(2,1)} %copy.58), calls=%async_computation.3 | async-start | bytes 2097152 | tf_op jit(solution)/shard_map/all_to_all | solution.py:206
  180.6 13.5 %reduce-scatter.3.cloned.1.call-done = bf16[32,2048]{1,0:T(8,128)(2,1)} async-done(((bf16[128,2048]{1,0:T(8,128)(2,1)}), bf16[32,2048]{1,0:T(8,128)(2,1)}) %reduce-scatter.3.cloned.1.call-update) | async-done | bytes 131088 | tf_op jit(solution)/shard_map/reduce_scatter | solution.py:146
  196.8 7.5 %all-to-all-done.1 = bf16[32,8,2048]{2,0,1:T(8,128)(2,1)} async-done(((bf16[32,8,2048]{2,0,1:T(8,128)(2,1)}), bf16[32,8,2048]{2,0,1:T(8,128)(2,1)}, u32[]{:S(2)}, u32[]{:S(2)}) %all-to-all-start.1) | async-done | bytes 1048608 | tf_op jit(solution)/shard_map/all_to_all | solution.py:206
  204.3 2.8 %copy.68 = bf16[32,8,2048]{2,1,0:T(8,128)(2,1)} copy(bf16[32,8,2048]{2,0,1:T(8,128)(2,1)} %all-to-all-done.1) | data formatting | bytes 2097152 | tf_op jit(solution)/shard_map/all_to_all | solution.py:206
  207.2 3.6 %gather_fusion.1 = bf16[128,2048]{1,0:T(8,128)(2,1)} fusion(bf16[256,2048]{1,0:T(8,128)(2,1)} %bitcast.78, s32[1024]{0:T(1024)S(1)} %pad_clamp_fusion), kind=kCustom, calls=%fused_computation.1 | custom fusion | bytes 1049088 | tf_op jit(solution)/shard_map/gather | solution.py:211
  210.8 2.4 %reshape.248 = f32[32,4,2048]{2,1,0:T(4,128)} reshape(bf16[128,2048]{1,0:T(8,128)(2,1)} %gather_fusion.1) | data formatting | bytes 1572864 | tf_op jit(solution)/shard_map/convert_element_type | solution.py:212
  213.1 2.6 %multiply_reduce_fusion = bf16[32,2048]{1,0:T(8,128)(2,1)} fusion(f32[32,4,2048]{2,1,0:T(4,128)} %reshape.248, f32[32,4]{1,0:T(8,128)S(1)} %copy.60), kind=kLoop, calls=%fused_computation.42 | loop fusion | flops 458752 | bytes 1180160 | tf_op jit(solution)/shard_map/reduce_sum | solution.py:216
  (86 shorter events, 34.3 us)
Async XLA Ops:
  8.0 148.2 %copy-start = (bf16[2048,768]{1,0:T(8,128)(2,1)S(1)}, bf16[2048,768]{1,0:T(8,128)(2,1)}, u32[]{:S(2)}) copy-start(bf16[2048,768]{1,0:T(8,128)(2,1)} %param.21) | copy-start | bytes 9437188
  8.0 151.3 %all-gather.2.cloned.1.call-start = ((), (), s32[]{:S(2)}) async-start(), calls=%async_computation.4 | async-start | bytes 1179648 | tf_op jit(solution)/shard_map/all_gather | solution.py:134
  17.5 71.6 %copy-start.7 = (f32[2048]{0:T(1024)S(1)}, f32[2048]{0:T(1024)}, u32[]{:S(2)}) copy-start(f32[2048]{0:T(1024)} %param.20) | copy-start | bytes 24580
  17.5 74.0 %copy-start.8 = (f32[512]{0:T(512)S(1)}, f32[512]{0:T(512)}, u32[]{:S(2)}) copy-start(f32[512]{0:T(512)} %param.24) | copy-start | bytes 6148
  56.7 1.0 copy-start.1
  58.2 14.3 %collective-permute-start = (bf16[32,8,2048]{2,1,0:T(8,128)(2,1)S(1)}, bf16[32,8,2048]{2,1,0:T(8,128)(2,1)S(1)}, u32[]{:S(2)}, u32[]{:S(2)}) collective-permute-start(bf16[32,8,2048]{2,1,0:T(8,128)(2,1)S(1)} %copy.55), channel_id=1, source_target_pairs={{0,1},{1,2},{2,3},{3,0},{4,5},{5,6},{6,7},{7,4},{8,9},{9,10},{10,1... | collective-permute-start | bytes 3145736 | tf_op jit(solution)/shard_map/ppermute | solution.py:183
  72.5 1.0 copy-start.3
  73.6 14.3 %collective-permute-start.1 = (bf16[32,8,2048]{2,1,0:T(8,128)(2,1)S(1)}, bf16[32,8,2048]{2,1,0:T(8,128)(2,1)}, u32[]{:S(2)}, u32[]{:S(2)}) collective-permute-start(bf16[32,8,2048]{2,1,0:T(8,128)(2,1)S(1)} %collective-permute-done), channel_id=1, source_target_pairs={{0,1},{1,2},{2,3},{3,0},{4,5},{5,6},{6,7},{7,4},{8,9},{9,10},{10,1... | collective-permute-start | bytes 3145736 | tf_op jit(solution)/shard_map/ppermute | solution.py:183
  87.9 14.5 %collective-permute-start.2 = (bf16[32,8,2048]{2,1,0:T(8,128)(2,1)}, bf16[32,8,2048]{2,1,0:T(8,128)(2,1)}, u32[]{:S(2)}, u32[]{:S(2)}) collective-permute-start(bf16[32,8,2048]{2,1,0:T(8,128)(2,1)} %collective-permute-done.1), channel_id=1, source_target_pairs={{0,1},{1,2},{2,3},{3,0},{4,5},{5,6},{6,7},{7,4},{8,9},{9,10},{10,1... | collective-permute-start | bytes 3145736 | tf_op jit(solution)/shard_map/ppermute | solution.py:183
  92.3 80.9 %reduce-scatter.5.cloned.1.call-start = ((), (), s32[]{:S(2)}) async-start(), calls=%async_computation.6 | async-start | bytes 5242880 | tf_op jit(solution)/shard_map/reduce_scatter | solution.py:197
  92.5 18.2 %copy-start.4 = (bf16[32,8,2048]{2,1,0:T(8,128)(2,1)S(1)}, bf16[32,8,2048]{2,1,0:T(8,128)(2,1)}, u32[]{:S(2)}) copy-start(bf16[32,8,2048]{2,1,0:T(8,128)(2,1)} %copy-done.3) | copy-start | bytes 3145732
  92.5 18.3 %copy-start.2 = (bf16[32,8,2048]{2,0,1:T(8,128)(2,1)S(1)}, bf16[32,8,2048]{2,0,1:T(8,128)(2,1)}, u32[]{:S(2)}) copy-start(bf16[32,8,2048]{2,0,1:T(8,128)(2,1)} %copy-done.1) | copy-start | bytes 3145732
  92.5 22.1 %copy-start.9 = (bf16[1,2048,256]{2,1,0:T(8,128)(2,1)S(1)}, bf16[1,2048,256]{2,1,0:T(8,128)(2,1)}, u32[]{:S(2)}) copy-start(bf16[1,2048,256]{2,1,0:T(8,128)(2,1)} %param.31) | copy-start | bytes 3145732
  111.4 3.2 %copy-start.5 = (bf16[256,8,2048]{2,1,0:T(8,128)(2,1)}, bf16[256,8,2048]{2,1,0:T(8,128)(2,1)S(1)}, u32[]{:S(2)}) copy-start(bf16[256,8,2048]{2,1,0:T(8,128)(2,1)S(1)} %constant_dynamic-update-slice_fusion) | copy-start | bytes 25165828
  116.9 9.6 %copy-start.10 = (bf16[2048,64]{0,1:T(8,128)(2,1)S(1)}, bf16[2048,64]{0,1:T(8,128)(2,1)}, u32[]{:S(2)}) copy-start(bf16[2048,64]{0,1:T(8,128)(2,1)} %param.23) | copy-start | bytes 786436
  126.4 67.7 %reduce-scatter.3.cloned.1.call-start = ((), (), s32[]{:S(2)}) async-start(), calls=%async_computation.5 | async-start | bytes 655360 | tf_op jit(solution)/shard_map/reduce_scatter | solution.py:146
  159.3 21.0 %copy-start.6 = (f32[128,4]{0,1:T(4,128)S(1)}, f32[128,4]{0,1:T(4,128)}, u32[]{:S(2)}) copy-start(f32[128,4]{0,1:T(4,128)} %param.35) | copy-start | bytes 6148
  176.1 28.3 %all-to-all-start.1 = ((bf16[32,8,2048]{2,0,1:T(8,128)(2,1)}), bf16[32,8,2048]{2,0,1:T(8,128)(2,1)}, u32[]{:S(2)}, u32[]{:S(2)}) async-start(bf16[32,8,2048]{2,0,1:T(8,128)(2,1)} %copy.58), calls=%async_computation.3 | async-start | bytes 2097152 | tf_op jit(solution)/shard_map/all_to_all | solution.py:206
Sparse Core Ops, SparseCore 0:
  92.4 39.6 all-gather.1
Sparse Core Ops, SparseCore 1:
  126.5 43.6 reduce-scatter.4
  173.3 20.8 reduce-scatter.2
